TPU v7x, 512 devices: a whole 4x8x8 slice. The times are simulated.
512 devices in a mesh: fs: 64 (over z, y), tp: 8 (over x, core).
Axes of the slice: x: 4, y: 8, z: 8, core: 2. Of those that a mesh axis runs over, the one named last changes fastest.
Arguments:
- saved_input: bfloat16 [65536, 2048], P('fs'), may hold values from -60 to 60
- out_cotangent: bfloat16 [65536, 4096], P('fs', 'tp'), may hold values from -6 to 6
- old_weight: float32 [2048, 4096], P('fs', 'tp'), may hold values from -0.125 to 0.125
- factor: bfloat16 [4096, 256], P('tp'), may hold values from -0.09375 to 0.09375
- moment_first: float32 [2048, 256], P('fs'), may hold values from -3 to 3
- moment_second: float32 [2048, 256], P('fs'), may hold values from 0.05 to 1
Outputs:
- new_weight: float32 [2048, 4096], P('fs', 'tp')
- update: float32 [2048, 4096], P('fs', 'tp')
- new_first: float32 [2048, 256], P('fs')
- new_second: float32 [2048, 256], P('fs')
- weight_copy: bfloat16 [2048, 4096], P(None, 'tp')
All inputs are finite; a program needn't handle non-finite values.
Results may differ from a plain program's by a relative error of at most 0.0028.
Values may be sent and summed in bfloat16 or wider, within the bound.
No kernel may reach another device: no remote copies, remote signals or barrier semaphores. Data moves between devices by JAX's collectives and lax.ppermute only.
A program may use at most 64 MiB of HBM per device.

v0:
```python
import math
import jax
import jax.numpy as jnp
from jax import lax
from jax.sharding import Mesh
from jax.sharding import PartitionSpec as P

HV = 2048
RANK = 256
FS = ("fs_0", "fs_1")


def in_blocks(shard, dim, devices):
    before, after = (shard.shape[:dim], shard.shape[dim + 1 :])
    return jnp.moveaxis(shard.reshape(*before, devices, -1, *after), dim, 0)


def sent_and_summed(shard, axis, dim):
    devices = lax.axis_size(axis)
    tiles = lax.all_to_all(in_blocks(shard, dim, devices), axis, 0, 0, tiled=True)
    return jnp.sum(tiles.astype(jnp.float32), axis=0)


def copy_for_each(shard, axis):
    devices = lax.axis_size(axis)
    return lax.all_to_all(
        jnp.broadcast_to(shard[None], (devices, *shard.shape)), axis, 0, 0, tiled=True
    )


def taken_together(shard, axis):
    return copy_for_each(shard, axis).sum(axis=0)


def one_axis_at_a_time(shard, axes):
    for axis in axes:
        shard = lax.psum(shard, axis)
    return shard


def laid_out(tiles, dim):
    tiles = jnp.moveaxis(tiles, 0, dim)
    dims = tiles.shape
    return tiles.reshape(*dims[:dim], dims[dim] * dims[dim + 1], *dims[dim + 2 :])


def stacked_from(shard, axes, order):
    tiles = shard[None]
    for k in order:
        tiles = lax.all_gather(tiles, axes[k], axis=0, tiled=True)
    held = [lax.axis_size(axes[k]) for k in reversed(order)]
    tiles = tiles.reshape(*held, *shard.shape)
    turned = sorted(range(len(order)), key=lambda place: order[len(order) - 1 - place])
    return tiles.transpose(*turned, *range(len(order), tiles.ndim)).reshape(-1, *shard.shape)


def whole_of(shard, axes, order, dim):
    return laid_out(stacked_from(shard, axes, order), dim)


def on_device(saved_input, out_cotangent, old_weight, factor, moment_first, moment_second):
    wide_factor = factor.astype(jnp.float32)
    contract = (((0,), (0,)), ((), ()))
    gradient = sent_and_summed(
        lax.dot_general(
            saved_input, out_cotangent, contract, preferred_element_type=jnp.float32
        ).astype(jnp.bfloat16),
        FS,
        0,
    )
    partial_low = jnp.dot(gradient, wide_factor, precision=lax.Precision.HIGHEST)
    projected = taken_together(partial_low, "tp")
    squares = one_axis_at_a_time(jnp.sum(projected * projected), FS)
    clip = jnp.minimum(1.0, math.sqrt(HV * RANK) / (jnp.sqrt(squares) + 1e-06))
    clipped = clip * projected
    new_first = 0.9 * moment_first + 0.1 * clipped
    new_second = 0.95 * moment_second + 0.05 * clipped * clipped
    direction = new_first / (jnp.sqrt(new_second) + 1e-08)
    update = jnp.dot(direction, wide_factor.T, precision=lax.Precision.HIGHEST)
    new_weight = old_weight - 0.05 * update
    copied = whole_of(new_weight.astype(jnp.bfloat16), FS, (0, 1), 0)
    return (new_weight, update, new_first, new_second, copied)


def solution(mesh):
    finer = Mesh(mesh.devices.reshape(8, 8, mesh.shape["tp"]), ("fs_0", "fs_1", "tp"))
    in_specs = (P(FS, None), P(FS, "tp"), P(FS, "tp"), P("tp", None), P(FS, None), P(FS, None))
    out_specs = (P(FS, "tp"), P(FS, "tp"), P(FS, None), P(FS, None), P(None, "tp"))
    return jax.shard_map(
        on_device, mesh=finer, in_specs=in_specs, out_specs=out_specs, check_vma=False
    )
```

profile of v0, /device:TPU:2, one launch (start us, length us, event | category | flops | bytes accessed | tf_op | source)
XLA Modules:
  0.0 204.9 jit_solution(14049241271818606529)
XLA Ops:
  7.2 0.0 copy-start
  7.2 0.0 all-gather.3.cloned.1.call-start
  7.2 1.2 copy-done
  8.4 4.6 %convolution_convert_fusion = bf16[2048,512]{1,0:T(8,128)(2,1)S(1)} fusion(bf16[1024,2048]{1,0:T(8,128)(2,1)} %param.6, bf16[1024,512]{1,0:T(8,128)(2,1)S(1)} %copy-done), kind=kOutput, calls=%fused_computation.1 | convolution fusion | flops 2148532224 | bytes 7340032 | tf_op jit(solution)/shard_map/dot_general | solution.py:65
  13.0 0.0 copy-start.1
  13.0 0.0 copy-start.5
  13.0 0.0 copy-start.6
  13.0 0.0 copy-start.4
  13.0 68.7 %all_to_all.10 = bf16[64,32,512]{2,1,0:T(8,128)(2,1)S(1)} all-to-all(bf16[64,32,512]{2,1,0:T(8,128)(2,1)S(1)} %bitcast.13), channel_id=1, replica_groups=mesh['fs_0'=8,'fs_1'=8,'tp'=8] {'fs_0','fs_1'}, dimensions={0} | all-to-all | bytes 4194304 | tf_op jit(solution)/shard_map/all_to_all | solution.py:20
  81.7 0.3 convert_reduce_fusion
  82.0 0.0 copy-done.1
  82.0 0.2 fusion.8
  82.3 10.7 %all_to_all.11 = f32[8,32,256]{2,1,0:T(8,128)S(1)} all-to-all(f32[8,32,256]{2,1,0:T(8,128)S(1)} %broadcast_in_dim.4), channel_id=1, replica_groups=mesh['fs_0'=8,'fs_1'=8,'tp'=8] {'tp'}, dimensions={0} | all-to-all | bytes 524288 | tf_op jit(solution)/shard_map/all_to_all | solution.py:26
  93.0 0.6 multiply_reduce_fusion
  93.6 16.6 %psum.14 = f32[]{:T(128)} all-reduce(f32[]{:T(128)} %multiply_reduce_fusion), channel_id=1, replica_groups=mesh['fs_0'=8,'fs_1'=8,'tp'=8] {'fs_0'}, use_global_device_ids=true, to_apply=%region_3.0 | all-reduce | flops 1 | bytes 8 | tf_op jit(solution)/shard_map/psum | solution.py:37
  110.2 16.5 %psum.15 = f32[]{:T(128)} all-reduce(f32[]{:T(128)} %psum.14), channel_id=1, replica_groups=mesh['fs_0'=8,'fs_1'=8,'tp'=8] {'fs_1'}, use_global_device_ids=true, to_apply=%region_4.0 | all-reduce | flops 1 | bytes 8 | tf_op jit(solution)/shard_map/psum | solution.py:37
  127.5 0.0 copy-done.5
  127.5 0.0 copy-done.6
  127.5 0.0 copy-start.2
  127.5 0.0 copy-start.3
  127.5 0.0 copy-done.4
  127.5 1.0 fusion.7
  128.5 26.8 %all-gather = bf16[256,512]{1,0:T(8,128)(2,1)} all-gather(bf16[32,512]{1,0:T(8,128)(2,1)S(1)} %get-tuple-element.5), channel_id=2, replica_groups=mesh['fs_0'=8,'fs_1'=8,'tp'=8] {'fs_0'}, dimensions={0}, use_global_device_ids=true | all-gather | bytes 294912 | tf_op jit(solution)/shard_map/all_gather | solution.py:50
  155.4 0.0 all-gather.3.cloned.1.call-update
  155.4 39.5 %all-gather.3.cloned.1.call-done = bf16[64,32,512]{2,1,0:T(8,128)(2,1)} async-done(((bf16[8,32,512]{2,1,0:T(8,128)(2,1)}), bf16[64,32,512]{2,1,0:T(8,128)(2,1)}) %all-gather.3.cloned.1.call-update) | async-done | bytes 2097168 | tf_op jit(solution)/shard_map/all_gather | solution.py:50
  194.9 3.2 %copy.13 = bf16[8,8,32,512]{3,2,1,0:T(8,128)(2,1)} copy(bf16[8,8,32,512]{3,2,0,1:T(8,128)(2,1)} %bitcast.12) | data formatting | bytes 4194304 | tf_op jit(solution)/shard_map/transpose | solution.py:54
  198.1 0.0 copy-done.2
  198.1 0.0 copy-done.3
  (3 shorter events, 0.1 us)
Async XLA Ops:
  7.2 1.2 copy-start
  7.2 187.7 %all-gather.3.cloned.1.call-start = ((), (), s32[]{:S(2)}) async-start(), calls=%async_computation.2 | async-start | bytes 2359296 | tf_op jit(solution)/shard_map/all_gather | solution.py:50
  13.0 69.1 %copy-start.1 = (bf16[512,256]{1,0:T(8,128)(2,1)S(1)}, bf16[512,256]{1,0:T(8,128)(2,1)}, u32[]{:S(2)}) copy-start(bf16[512,256]{1,0:T(8,128)(2,1)} %param.9) | copy-start | bytes 786436
  13.0 114.5 %copy-start.5 = (f32[32,256]{1,0:T(8,128)S(1)}, f32[32,256]{1,0:T(8,128)}, u32[]{:S(2)}) copy-start(f32[32,256]{1,0:T(8,128)} %param.11) | copy-start | bytes 98308
  13.0 114.5 %copy-start.6 = (f32[32,256]{1,0:T(8,128)S(1)}, f32[32,256]{1,0:T(8,128)}, u32[]{:S(2)}) copy-start(f32[32,256]{1,0:T(8,128)} %param.10) | copy-start | bytes 98308
  13.0 114.5 %copy-start.4 = (f32[32,512]{1,0:T(8,128)S(1)}, f32[32,512]{1,0:T(8,128)}, u32[]{:S(2)}) copy-start(f32[32,512]{1,0:T(8,128)} %param.8) | copy-start | bytes 196612
  127.5 70.6 %copy-start.2 = (f32[32,256]{1,0:T(8,128)}, f32[32,256]{1,0:T(8,128)S(1)}, u32[]{:S(2)}) copy-start(f32[32,256]{1,0:T(8,128)S(1)} %get-tuple-element.7) | copy-start | bytes 98308
  127.5 70.6 %copy-start.3 = (f32[32,256]{1,0:T(8,128)}, f32[32,256]{1,0:T(8,128)S(1)}, u32[]{:S(2)}) copy-start(f32[32,256]{1,0:T(8,128)S(1)} %get-tuple-element.8) | copy-start | bytes 98308
Sparse Core Ops, SparseCore 0:
  155.5 39.3 all-gather.2
where the time goes:
time: 205 us
  blocking collectives  139 us (68%)
  waiting for transfers between devices  39.5 us (19%)
  between operations  14.9 us (7%)
  matrix products  5.81 us (3%)
  local copies, waits for them, and re-layouts  4.39 us (2%)
    all_to_all x1, blocking collectives, sent_and_summed(): lax.all_to_all(in_blocks(shard, dim, devices), axis, 0, 0, tiled=True)  68.7 us
    all_gather x1, waiting for transfers between devices, stacked_from(): tiles = lax.all_gather(tiles, axes[k], axis=0, tiled=True)  39.5 us
    psum x2, blocking collectives, one_axis_at_a_time(): shard = lax.psum(shard, axis)  33.1 us
    all_gather x1, blocking collectives, stacked_from(): tiles = lax.all_gather(tiles, axes[k], axis=0, tiled=True)  26.8 us
    all_to_all x1, blocking collectives, copy_for_each(): lax.all_to_all(jnp.broadcast_to(shard[None], (devices, *shard.shape)), ax...  10.7 us
    dot_general x1, matrix products, on_device(): lax.dot_general(saved_input, out_cotangent, contract, preferred_element_t...  4.56 us
  transfers between devices with their start and end apart: 1, of which 1 were waited for; matrix products, arithmetic and copies ran while one was open for 0% of the time, Pallas kernels for 0%

commit v1 on v0

--- a/solution.py
+++ b/solution.py
@@ -47,7 +47,10 @@
 def stacked_from(shard, axes, order):
     tiles = shard[None]
     for k in order:
-        tiles = lax.all_gather(tiles, axes[k], axis=0, tiled=True)
+        incoming_x = axes[k]
+        tiles = jnp.concatenate(
+            lax.all_to_all(jnp.stack(lax.axis_size(incoming_x) * [tiles]), incoming_x, 0, 0), 0
+        )
     held = [lax.axis_size(axes[k]) for k in reversed(order)]
     tiles = tiles.reshape(*held, *shard.shape)
     turned = sorted(range(len(order)), key=lambda place: order[len(order) - 1 - place])

time: 205 us -> 186 us (0.907)
  waiting for transfers between devices: 39.5 us -> 0 us
  blocking collectives: 139 us -> 174 us
  between operations: 14.9 us -> 1.47 us
    all_to_all x0 -> x2, blocking collectives: none -> 61.7 us  [stacked_from(): lax.all_to_all(jnp.stack(lax.axis_size(incoming_x) * [tiles]), incoming_x...]
    all_gather x1 -> x0, waiting for transfers between devices: 39.5 us -> none  [stacked_from(): tiles = lax.all_gather(tiles, axes[k], axis=0, tiled=True)]
    all_gather x1 -> x0, blocking collectives: 26.8 us -> none  [stacked_from(): tiles = lax.all_gather(tiles, axes[k], axis=0, tiled=True)]
    transpose x1 -> x0, local copies, waits for them, and re-layouts: 3.16 us -> none  [stacked_from(): tiles.transpose(*turned, *range(len(order), tiles.ndim))]
  transfers between devices with their start and end apart: 1 -> 0, of which waited for: 1 -> 0; matrix products, arithmetic and copies ran while one was open for 0% -> 0% of each run, Pallas kernels for 0% -> 0%
where the time goes in v1:
time: 186 us
  blocking collectives  174 us (94%)
  matrix products  5.81 us (3%)
  local copies, waits for them, and re-layouts  3.7 us (2%)
    all_to_all x1, blocking collectives, sent_and_summed(): lax.all_to_all(in_blocks(shard, dim, devices), axis, 0, 0, tiled=True)  68.5 us
    all_to_all x2, blocking collectives, stacked_from(): lax.all_to_all(jnp.stack(lax.axis_size(incoming_x) * [tiles]), incoming_x...  61.7 us
    psum x2, blocking collectives, one_axis_at_a_time(): shard = lax.psum(shard, axis)  33.1 us
    all_to_all x1, blocking collectives, copy_for_each(): lax.all_to_all(jnp.broadcast_to(shard[None], (devices, *shard.shape)), ax...  10.7 us
    dot_general x1, matrix products, on_device(): lax.dot_general(saved_input, out_cotangent, contract, preferred_element_t...  4.56 us

profile of v1, /device:TPU:2, one launch (start us, length us, event | category | flops | bytes accessed | tf_op | source)
XLA Modules:
  0.0 186.0 jit_solution(15490089011415035420)
XLA Ops:
  0.6 0.0 copy-start
  0.6 1.2 copy-done
  1.9 4.6 %convolution_convert_fusion = bf16[2048,512]{1,0:T(8,128)(2,1)S(1)} fusion(bf16[1024,2048]{1,0:T(8,128)(2,1)} %param.6, bf16[1024,512]{1,0:T(8,128)(2,1)S(1)} %copy-done), kind=kOutput, calls=%fused_computation.1 | convolution fusion | flops 2148532224 | bytes 7340032 | tf_op jit(solution)/shard_map/dot_general | solution.py:68
  6.4 68.5 %all_to_all.20 = bf16[64,32,512]{2,1,0:T(8,128)(2,1)S(1)} all-to-all(bf16[64,32,512]{2,1,0:T(8,128)(2,1)S(1)} %bitcast.11), channel_id=1, replica_groups=mesh['fs_0'=8,'fs_1'=8,'tp'=8] {'fs_0','fs_1'}, dimensions={0} | all-to-all | bytes 4194304 | tf_op jit(solution)/shard_map/all_to_all | solution.py:20
  75.0 0.0 copy-start.1
  75.0 0.0 copy-start.5
  75.0 0.0 copy-start.6
  75.0 0.0 copy-start.4
  75.0 0.3 convert_reduce_fusion
  75.3 0.6 copy-done.1
  75.9 0.2 fusion.8
  76.2 10.7 %all_to_all.21 = f32[8,32,256]{2,1,0:T(8,128)S(1)} all-to-all(f32[8,32,256]{2,1,0:T(8,128)S(1)} %broadcast_in_dim.2), channel_id=1, replica_groups=mesh['fs_0'=8,'fs_1'=8,'tp'=8] {'tp'}, dimensions={0} | all-to-all | bytes 524288 | tf_op jit(solution)/shard_map/all_to_all | solution.py:26
  86.9 0.6 multiply_reduce_fusion
  87.5 16.6 %psum.14 = f32[]{:T(128)} all-reduce(f32[]{:T(128)} %multiply_reduce_fusion), channel_id=1, replica_groups=mesh['fs_0'=8,'fs_1'=8,'tp'=8] {'fs_0'}, use_global_device_ids=true, to_apply=%region_3.0 | all-reduce | flops 1 | bytes 8 | tf_op jit(solution)/shard_map/psum | solution.py:37
  104.1 16.5 %psum.15 = f32[]{:T(128)} all-reduce(f32[]{:T(128)} %psum.14), channel_id=1, replica_groups=mesh['fs_0'=8,'fs_1'=8,'tp'=8] {'fs_1'}, use_global_device_ids=true, to_apply=%region_4.0 | all-reduce | flops 1 | bytes 8 | tf_op jit(solution)/shard_map/psum | solution.py:37
  121.4 0.0 copy-done.5
  121.4 0.0 copy-done.6
  121.4 0.0 copy-start.2
  121.4 0.0 copy-start.3
  121.4 0.0 copy-done.4
  121.4 1.0 fusion.7
  122.5 15.2 %all_to_all.22 = bf16[8,1,32,512]{3,2,1,0:T(8,128)(2,1)S(1)} all-to-all(bf16[8,1,32,512]{3,2,1,0:T(8,128)(2,1)S(1)} %stack.6), channel_id=1, replica_groups=mesh['fs_0'=8,'fs_1'=8,'tp'=8] {'fs_0'}, dimensions={0} | all-to-all | bytes 524288 | tf_op jit(solution)/shard_map/all_to_all | solution.py:52
  137.6 0.2 stack.7
  137.9 46.6 %all_to_all.23 = bf16[8,8,32,512]{3,2,1,0:T(8,128)(2,1)S(1)} all-to-all(bf16[8,8,32,512]{3,2,1,0:T(8,128)(2,1)S(1)} %stack.7), channel_id=1, replica_groups=mesh['fs_0'=8,'fs_1'=8,'tp'=8] {'fs_1'}, dimensions={0} | all-to-all | bytes 4194304 | tf_op jit(solution)/shard_map/all_to_all | solution.py:52
  184.5 0.0 copy-done.2
  184.5 0.0 copy-done.3
  184.5 1.6 copy.12
  (4 shorter events, 0.1 us)
Async XLA Ops:
  0.6 1.2 copy-start
  75.0 1.0 copy-start.1
  75.0 46.4 %copy-start.5 = (f32[32,256]{1,0:T(8,128)S(1)}, f32[32,256]{1,0:T(8,128)}, u32[]{:S(2)}) copy-start(f32[32,256]{1,0:T(8,128)} %param.11) | copy-start | bytes 98308
  75.0 46.4 %copy-start.6 = (f32[32,256]{1,0:T(8,128)S(1)}, f32[32,256]{1,0:T(8,128)}, u32[]{:S(2)}) copy-start(f32[32,256]{1,0:T(8,128)} %param.10) | copy-start | bytes 98308
  75.0 46.4 %copy-start.4 = (f32[32,512]{1,0:T(8,128)S(1)}, f32[32,512]{1,0:T(8,128)}, u32[]{:S(2)}) copy-start(f32[32,512]{1,0:T(8,128)} %param.8) | copy-start | bytes 196612
  121.4 63.1 %copy-start.2 = (f32[32,256]{1,0:T(8,128)}, f32[32,256]{1,0:T(8,128)S(1)}, u32[]{:S(2)}) copy-start(f32[32,256]{1,0:T(8,128)S(1)} %get-tuple-element.7) | copy-start | bytes 98308
  121.4 63.1 %copy-start.3 = (f32[32,256]{1,0:T(8,128)}, f32[32,256]{1,0:T(8,128)S(1)}, u32[]{:S(2)}) copy-start(f32[32,256]{1,0:T(8,128)S(1)} %get-tuple-element.8) | copy-start | bytes 98308
